TPU v7x, 32 devices: a whole 2x2x4 slice. The times are simulated.
32 devices in a mesh: sp: 8 (over z, y), tp: 4 (over x, core).
Axes of the slice: x: 2, y: 2, z: 4, core: 2. Of those that a mesh axis runs over, the one named last changes fastest.
Arguments:
- queries: bfloat16 [4096, 1024], P('sp', 'tp'), may hold values from -200 to 200
- keys: bfloat16 [4096, 1024], P('sp', 'tp'), may hold values from -6 to 6
- values: bfloat16 [4096, 1024], P('sp', 'tp'), may hold values from -24 to 24
- cum_gate: float32 [4096, 8], P('sp', 'tp'), may hold values from -414 to 0, as said below
- residual: bfloat16 [4096, 2048], P(('sp', 'tp')), may hold values from -1.5 to 1.5
- w_out: bfloat16 [1024, 2048], replicated, may hold values from -0.1875 to 0.1875
- gain: float32 [2048], replicated, may hold values from 0.1 to 1.9
- w_up: bfloat16 [2048, 8192], P('sp', 'tp'), may hold values from -0.125 to 0.125
- w_down: bfloat16 [8192, 2048], P('tp', 'sp'), may hold values from -0.0625 to 0.0625
Outputs:
- output: bfloat16 [4096, 2048], P(('sp', 'tp'))
Inputs may be any that keep to these rules, and one draw needn't show every extreme that they name: Within each head, cum_gate never rises from one position to the next.
All inputs are finite; a program needn't handle non-finite values.
Results may differ from a plain program's by a relative error of at most 0.022.
Values may be sent and summed in bfloat16 or wider, within the bound.
A program may use at most 128 MiB of HBM per device.

v0:
```python
import math
import jax
import jax.numpy as jnp
from jax import lax
from jax.sharding import PartitionSpec as P


def per_device(queries, keys, values, cum_gate, residual, w_out, gain, w_up, w_down):
    tok_rows, width = queries.shape
    heads_here = cum_gate.shape[1]
    head_size = width // heads_here
    score_scale = head_size ** (-0.5)
    row_offset = lax.axis_index("sp") * tok_rows
    query_heads = queries.reshape(tok_rows, heads_here, head_size)
    query_pos = row_offset + jnp.arange(tok_rows, dtype=jnp.int32)
    all_gates = lax.all_gather(cum_gate, "sp", axis=0, tiled=True)
    initial = (
        jnp.full((tok_rows, heads_here), -1e30, jnp.float32),
        jnp.zeros((tok_rows, heads_here), jnp.float32),
        jnp.zeros((tok_rows, heads_here, head_size), jnp.float32),
    )
    carried = initial
    key_rows = lax.all_gather(keys, "sp", axis=0, tiled=True)
    value_rows = lax.all_gather(values, "sp", axis=0, tiled=True)
    row_count = key_rows.shape[0]
    span_rows = math.gcd(row_count, 2048)
    block_count = row_count // span_rows
    key_blocks = key_rows.reshape(block_count, span_rows, heads_here, head_size)
    value_blocks = value_rows.reshape(block_count, span_rows, heads_here, head_size)
    first_pos = jnp.arange(block_count, dtype=jnp.int32) * span_rows

    def absorb_block(running, packed):
        running_max, running_sum, accumulated = running
        key_blk, value_blk, block_start = packed
        gate_blk = lax.dynamic_slice_in_dim(all_gates, block_start, span_rows, 0)
        scores = jnp.einsum(
            "qhd,khd->qhk", query_heads, key_blk, preferred_element_type=jnp.float32
        )
        scores = scores * score_scale + cum_gate[:, :, None] - gate_blk.T[None, :, :]
        key_pos = block_start + jnp.arange(span_rows, dtype=jnp.int32)
        scores = jnp.where(key_pos[None, None, :] <= query_pos[:, None, None], scores, -1e30)
        new_max = jnp.maximum(running_max, jnp.max(scores, axis=-1))
        rescale = jnp.exp(running_max - new_max)
        weights = jnp.exp(scores - new_max[:, :, None])
        running_sum = running_sum * rescale + jnp.sum(weights, axis=-1)
        product = jnp.einsum(
            "qhk,khd->qhd",
            weights.astype(jnp.bfloat16),
            value_blk,
            preferred_element_type=jnp.float32,
        )
        accumulated = accumulated * rescale[:, :, None] + product
        return ((new_max, running_sum, accumulated), None)

    carried, _ = lax.scan(absorb_block, carried, (key_blocks, value_blocks, first_pos))
    running_max, running_sum, accumulated = carried
    attended = (accumulated / running_sum[:, :, None]).reshape(tok_rows, width).astype(jnp.bfloat16)
    mine = lax.all_to_all(attended, "tp", split_axis=0, concat_axis=1, tiled=True)
    projected = jnp.dot(mine, w_out, preferred_element_type=jnp.float32)
    residual_sum = residual.astype(jnp.float32) + projected
    mean_square = jnp.mean(residual_sum * residual_sum, axis=-1, keepdims=True)
    normed = (residual_sum * lax.rsqrt(mean_square + 1e-06) * gain).astype(jnp.bfloat16)
    normed_all = lax.all_gather(normed, "tp", axis=0, tiled=True)
    up_proj = jnp.dot(
        normed_all,
        lax.all_gather(w_up, "sp", axis=0, tiled=True),
        preferred_element_type=jnp.float32,
    )
    hidden = jnp.square(jax.nn.relu(up_proj)).astype(jnp.bfloat16)
    down_whole = lax.all_gather(w_down, "sp", axis=1, tiled=True)
    rounded = jnp.dot(hidden, down_whole, preferred_element_type=jnp.float32).astype(jnp.bfloat16)
    branch_out = lax.psum_scatter(
        lax.optimization_barrier(rounded).astype(jnp.float32).astype(jnp.bfloat16),
        "tp",
        scatter_dimension=0,
        tiled=True,
    ).astype(jnp.float32)
    return (residual_sum + branch_out).astype(jnp.bfloat16)


def solution(mesh):
    return jax.shard_map(
        per_device,
        mesh=mesh,
        in_specs=(
            P("sp", "tp"),
            P("sp", "tp"),
            P("sp", "tp"),
            P("sp", "tp"),
            P(("sp", "tp"), None),
            P(),
            P(),
            P("sp", "tp"),
            P("tp", "sp"),
        ),
        out_specs=P(("sp", "tp"), None),
        check_vma=False,
    )
```

profile of v0, /device:TPU:0, one launch (start us, length us, event | category | flops | bytes accessed | tf_op | source)
XLA Modules:
  0.0 501.9 jit_solution(15590965651173478988)
XLA Ops:
  6.5 0.0 copy-start
  6.5 0.0 all-gather.6.cloned.1.call-start
  6.5 0.7 all-gather.6.cloned.1.call-update
  7.3 0.0 all-gather.8.cloned.1.call-start
  7.3 0.7 all-gather.8.cloned.1.call-update
  8.0 0.0 all-gather.10.cloned.1.call-start
  8.1 1.1 copy.17
  9.2 0.2 copy.19
  9.4 32.7 %all_gather.19 = f32[4096,2]{0,1:T(2,128)S(1)} all-gather(f32[512,2]{0,1:T(2,128)} %param.14), channel_id=1, replica_groups=mesh['sp'=8,'tp'=4] {'sp'}, dimensions={0}, use_global_device_ids=true | all-gather | bytes 36864 | tf_op jit(solution)/shard_map/all_gather | solution.py:16
  42.0 19.4 %all-gather.6.cloned.1.call-done = bf16[4096,256]{1,0:T(8,128)(2,1)} async-done(((bf16[512,256]{1,0:T(8,128)(2,1)}), bf16[4096,256]{1,0:T(8,128)(2,1)}) %all-gather.6.cloned.1.call-update) | async-done | bytes 2097168 | tf_op jit(solution)/shard_map/all_gather | solution.py:23
  61.4 4.0 reshape.62
  65.4 45.8 %all-gather.8.cloned.1.call-done = bf16[4096,256]{1,0:T(8,128)(2,1)} async-done(((bf16[512,256]{1,0:T(8,128)(2,1)}), bf16[4096,256]{1,0:T(8,128)(2,1)}) %all-gather.8.cloned.1.call-update) | async-done | bytes 2097168 | tf_op jit(solution)/shard_map/all_gather | solution.py:24
  111.2 4.0 reshape.64
  115.2 0.0 copy-done
  115.2 45.9 %while.15 = (s32[]{:T(128)}, f32[512,2]{0,1:T(2,128)S(1)}, f32[512,2]{0,1:T(2,128)S(1)}, f32[512,2,128]{0,2,1:T(8,128)}, s32[2]{0:T(128)S(1)}, /*index=5*/bf16[2...) while((s32[]{:T(128)}, f32[512,2]{0,1:T(2,128)S(1)}, ...), condition=%wide.region_3.4_spmd.clone, body=%wide.region_0.3_spmd.clone.sunk | while | flops 1110842880 | bytes 39239884 | solution.py:55
  115.2 0.6 dynamic_slice.26
  117.4 0.1 dynamic-slice_bitcast_fusion.2
  117.5 0.6 iota_add_fusion.5
  118.1 0.8 broadcast_compare_fusion.2
  118.9 2.7 constant_dynamic-slice_fusion.3
  121.6 4.6 fusion.40
  126.2 4.8 fusion.42
  131.0 0.8 copy.34
  131.8 6.2 %fusion.44 = f32[512,2,128]{0,2,1:T(8,128)} fusion(f32[2,2048,512]{2,1,0:T(8,128)} %get-tuple-element.231, f32[512,2]{0,1:T(2,128)S(1)} %fusion.41, f32[2,2048]{1,0:T(2,128)S(1)} %dynamic-slice_bitcast_fusion.2, f32[512,2]{0,1:T(2,128)S(1)} %get-tuple-element.270, pred[512,2048]{0,1:T(8,128)(4,1)S(1)} %broadcast_compare_fusion.2, ...), kind=kOutput, calls=%fused_computation.12.clone.1 | convolution fusion | flops 549847040 | bytes 11563009 | tf_op jit(solution)/shard_map/while/body/eval_jaxpr/qhk,khd->qhd/dot_general | solution.py:46
  138.1 0.6 dynamic_slice.26
  140.3 0.1 dynamic-slice_bitcast_fusion.2
  140.4 0.6 iota_add_fusion.5
  141.0 0.8 broadcast_compare_fusion.2
  141.8 2.7 constant_dynamic-slice_fusion.3
  144.5 4.6 fusion.40
  149.1 4.8 fusion.42
  153.9 0.8 copy.34
  154.7 6.4 %fusion.44 = f32[512,2,128]{0,2,1:T(8,128)} fusion(f32[2,2048,512]{2,1,0:T(8,128)} %get-tuple-element.231, f32[512,2]{0,1:T(2,128)S(1)} %fusion.41, f32[2,2048]{1,0:T(2,128)S(1)} %dynamic-slice_bitcast_fusion.2, f32[512,2]{0,1:T(2,128)S(1)} %get-tuple-element.270, pred[512,2048]{0,1:T(8,128)(4,1)S(1)} %broadcast_compare_fusion.2, ...), kind=kOutput, calls=%fused_computation.12.clone.1 | convolution fusion | flops 549847040 | bytes 11563009 | tf_op jit(solution)/shard_map/while/body/eval_jaxpr/qhk,khd->qhd/dot_general | solution.py:46
  161.1 0.0 copy-start.1
  161.1 1.1 divide_convert_fusion
  162.2 0.1 reshape.65
  162.2 0.2 copy.24
  162.4 8.5 %all_to_all.16 = bf16[4,128,256]{2,1,0:T(8,128)(2,1)S(1)} all-to-all(bf16[4,128,256]{2,1,0:T(8,128)(2,1)S(1)} %copy.24), channel_id=1, replica_groups=mesh['sp'=8,'tp'=4] {'tp'}, dimensions={0} | all-to-all | bytes 524288 | tf_op jit(solution)/shard_map/all_to_all | solution.py:58
  171.0 0.2 copy.22
  171.1 3.1 multiply_reduce_fusion
  174.3 0.0 copy-done.1
  174.3 0.9 multiply_convert_fusion.1
  175.2 0.0 all-gather.10.cloned.1.call-update
  175.3 0.0 all-gather.12.cloned.1.call-start
  175.3 0.5 all-gather.12.cloned.1.call-update
  175.8 0.0 all-gather.14.cloned.1.call-start
  175.9 0.5 all-gather.14.cloned.1.call-update
  176.4 0.2 reduce-scatter.2.cloned.1.call-start
  176.7 19.0 %all-gather.10.cloned.1.call-done = bf16[512,2048]{1,0:T(8,128)(2,1)} async-done(((bf16[128,2048]{1,0:T(8,128)(2,1)}), bf16[512,2048]{1,0:T(8,128)(2,1)}) %all-gather.10.cloned.1.call-update) | async-done | bytes 2097168 | tf_op jit(solution)/shard_map/all_gather | solution.py:63
  195.6 126.5 %all-gather.12.cloned.1.call-done = bf16[2048,2048]{1,0:T(8,128)(2,1)} async-done(((bf16[256,2048]{1,0:T(8,128)(2,1)}), bf16[2048,2048]{1,0:T(8,128)(2,1)}) %all-gather.12.cloned.1.call-update) | async-done | bytes 8388624 | tf_op jit(solution)/shard_map/all_gather | solution.py:66
  322.1 125.0 %all-gather.14.cloned.1.call-done = bf16[2048,2048]{1,0:T(8,128)(2,1)} async-done(((bf16[2048,256]{1,0:T(8,128)(2,1)}), bf16[2048,2048]{1,0:T(8,128)(2,1)}) %all-gather.14.cloned.1.call-update) | async-done | bytes 8388624 | tf_op jit(solution)/shard_map/all_gather | solution.py:70
  447.1 16.5 %convolution_convert_fusion = bf16[512,2048]{1,0:T(8,128)(2,1)} fusion(bf16[2048,2048]{1,0:T(8,128)(2,1)} %all-gather.14.cloned.1.call-done, bf16[512,2048]{1,0:T(8,128)(2,1)} %all-gather.10.cloned.1.call-done, bf16[2048,2048]{1,0:T(8,128)(2,1)} %all-gather.12.cloned.1.call-done), kind=kOutput, calls=%fused_computation.30 | convolution fusion | flops 8594128896 | bytes 20971520 | tf_op jit(solution)/shard_map/dot_general | solution.py:71
  463.7 0.0 reduce-scatter.2.cloned.1.call-update
  463.7 29.5 %reduce-scatter.2.cloned.1.call-done = bf16[128,2048]{1,0:T(8,128)(2,1)} async-done(((bf16[512,2048]{1,0:T(8,128)(2,1)}), bf16[128,2048]{1,0:T(8,128)(2,1)}) %reduce-scatter.2.cloned.1.call-update) | async-done | bytes 524304 | tf_op jit(solution)/shard_map/reduce_scatter | solution.py:72
  493.2 1.9 add_convert_fusion
  (13 shorter events, 0.1 us)
Async XLA Ops:
  6.5 108.6 %copy-start = (f32[512,2]{0,1:T(2,128)S(1)}, f32[512,2]{0,1:T(2,128)}, u32[]{:S(2)}) copy-start(f32[512,2]{0,1:T(2,128)} %param.14) | copy-start | bytes 12292
  6.5 54.9 %all-gather.6.cloned.1.call-start = ((), (), s32[]{:S(2)}) async-start(), calls=%async_computation.2 | async-start | bytes 2359296 | tf_op jit(solution)/shard_map/all_gather | solution.py:23
  7.3 103.9 %all-gather.8.cloned.1.call-start = ((), (), s32[]{:S(2)}) async-start(), calls=%async_computation.3 | async-start | bytes 2359296 | tf_op jit(solution)/shard_map/all_gather | solution.py:24
  8.0 187.6 %all-gather.10.cloned.1.call-start = ((), (), s32[]{:S(2)}) async-start(), calls=%async_computation.4 | async-start | bytes 2621440 | tf_op jit(solution)/shard_map/all_gather | solution.py:63
  161.1 13.2 %copy-start.1 = (f32[2048]{0:T(1024)S(1)}, f32[2048]{0:T(1024)}, u32[]{:S(2)}) copy-start(f32[2048]{0:T(1024)} %param.17) | copy-start | bytes 24580
  175.3 146.8 %all-gather.12.cloned.1.call-start = ((), (), s32[]{:S(2)}) async-start(), calls=%async_computation.5 | async-start | bytes 9437184 | tf_op jit(solution)/shard_map/all_gather | solution.py:66
  175.8 271.3 %all-gather.14.cloned.1.call-start = ((), (), s32[]{:S(2)}) async-start(), calls=%async_computation.6 | async-start | bytes 9437184 | tf_op jit(solution)/shard_map/all_gather | solution.py:70
  176.4 316.7 %reduce-scatter.2.cloned.1.call-start = ((), (), s32[]{:S(2)}) async-start(), calls=%async_computation.7 | async-start | bytes 2621440 | tf_op jit(solution)/shard_map/reduce_scatter | solution.py:72
Sparse Core Ops, SparseCore 0:
  9.5 51.9 all-gather.5
  63.5 47.6 all-gather.7
  175.4 20.1 all-gather.9
  197.6 124.4 all-gather.11
  324.0 123.1 all-gather.13
  463.8 29.3 reduce-scatter.1
where the time goes:
time: 502 us
  waiting for transfers between devices  368 us (73%)
  matrix products  41.4 us (8%)
  blocking collectives  41.2 us (8%)
  local copies, waits for them, and re-layouts  18 us (4%)
  other arithmetic  16.3 us (3%)
  between operations  13.6 us (3%)
    all_gather x1, waiting for transfers between devices, per_device(): lax.all_gather(w_up, 'sp', axis=0, tiled=True)  126 us
    all_gather x1, waiting for transfers between devices, per_device(): down_whole = lax.all_gather(w_down, 'sp', axis=1, tiled=True)  125 us
    all_gather x1, waiting for transfers between devices, per_device(): value_rows = lax.all_gather(values, 'sp', axis=0, tiled=True)  45.8 us
    all_gather x1, blocking collectives, per_device(): all_gates = lax.all_gather(cum_gate, 'sp', axis=0, tiled=True)  32.7 us
    reduce_scatter x1, waiting for transfers between devices, per_device(): lax.psum_scatter(lax.optimization_barrier(rounded).astype(jnp.float32).as...  29.5 us
    all_gather x1, waiting for transfers between devices, per_device(): key_rows = lax.all_gather(keys, 'sp', axis=0, tiled=True)  19.4 us
    all_gather x1, waiting for transfers between devices, per_device(): normed_all = lax.all_gather(normed, 'tp', axis=0, tiled=True)  19 us
    dot_general x1, matrix products, per_device(): jnp.dot(hidden, down_whole, preferred_element_type=jnp.float32)  16.5 us
  transfers between devices with their start and end apart: 6, of which 6 were waited for; matrix products, arithmetic and copies ran while one was open for 1% of the time, Pallas kernels for 0%

commit v1 on v0

--- a/solution.py
+++ b/solution.py
@@ -13,14 +13,17 @@
     row_offset = lax.axis_index("sp") * tok_rows
     query_heads = queries.reshape(tok_rows, heads_here, head_size)
     query_pos = row_offset + jnp.arange(tok_rows, dtype=jnp.int32)
-    all_gates = lax.all_gather(cum_gate, "sp", axis=0, tiled=True)
     initial = (
         jnp.full((tok_rows, heads_here), -1e30, jnp.float32),
         jnp.zeros((tok_rows, heads_here), jnp.float32),
         jnp.zeros((tok_rows, heads_here, head_size), jnp.float32),
     )
     carried = initial
-    key_rows = lax.all_gather(keys, "sp", axis=0, tiled=True)
+    all_gates, key_rows = jnp.split(
+        lax.all_gather(jnp.concatenate([cum_gate, keys], axis=1), "sp", axis=0, tiled=True),
+        [cum_gate.shape[1]],
+        axis=1,
+    )
     value_rows = lax.all_gather(values, "sp", axis=0, tiled=True)
     row_count = key_rows.shape[0]
     span_rows = math.gcd(row_count, 2048)

time: 502 us -> 547 us (1.090)
  waiting for transfers between devices: 368 us -> 423 us
  blocking collectives: 41.2 us -> 8.55 us
  local copies, waits for them, and re-layouts: 18 us -> 33.6 us
    all_gather x1, waiting for transfers between devices: 19.4 us -> 71.2 us  [per_device(): lax.all_gather(jnp.concatenate([cum_gate, keys], axis=1), 'sp', axis=0, t...]
    all_gather x1 -> x0, blocking collectives: 32.7 us -> none  [per_device(): all_gates = lax.all_gather(cum_gate, 'sp', axis=0, tiled=True)]
    dynamic_slice x6 -> x10, local copies, waits for them, and re-layouts: 8.16 us -> 21.1 us  [per_device(): lax.scan(absorb_block, carried, (key_blocks, value_blocks, first_pos))]
where the time goes in v1:
time: 547 us; the launch traced here: 546 us
  waiting for transfers between devices  423 us (77%)
  matrix products  45.5 us (8%)
  local copies, waits for them, and re-layouts  33.6 us (6%)
  other arithmetic  18 us (3%)
  between operations  13.6 us (2%)
  blocking collectives  8.55 us (2%)
    all_gather x1, waiting for transfers between devices, per_device(): lax.all_gather(w_up, 'sp', axis=0, tiled=True)  126 us
    all_gather x1, waiting for transfers between devices, per_device(): down_whole = lax.all_gather(w_down, 'sp', axis=1, tiled=True)  125 us
    all_gather x1, waiting for transfers between devices, per_device(): lax.all_gather(jnp.concatenate([cum_gate, keys], axis=1), 'sp', axis=0, t...  71.2 us
    all_gather x1, waiting for transfers between devices, per_device(): value_rows = lax.all_gather(values, 'sp', axis=0, tiled=True)  49.9 us
    reduce_scatter x1, waiting for transfers between devices, per_device(): lax.psum_scatter(lax.optimization_barrier(rounded).astype(jnp.float32).as...  29.5 us
    dynamic_slice x10, local copies, waits for them, and re-layouts, per_device(): lax.scan(absorb_block, carried, (key_blocks, value_blocks, first_pos))  21.1 us
    all_gather x1, waiting for transfers between devices, per_device(): normed_all = lax.all_gather(normed, 'tp', axis=0, tiled=True)  19.1 us
    dot_general x1, matrix products, per_device(): jnp.dot(hidden, down_whole, preferred_element_type=jnp.float32)  16.5 us
  transfers between devices with their start and end apart: 6, of which 6 were waited for; matrix products, arithmetic and copies ran while one was open for 1% of the time, Pallas kernels for 0%

profile of v1, /device:TPU:0, one launch (start us, length us, event | category | flops | bytes accessed | tf_op | source)
XLA Modules:
  0.0 546.1 jit_solution(1133121253935521033)
XLA Ops:
  6.5 0.0 all-gather.8.cloned.1.call-start
  6.5 0.0 copy-start
  6.5 0.7 all-gather.8.cloned.1.call-update
  7.3 0.0 all-gather.6.cloned.1.call-start
  7.3 1.1 copy.20
  8.4 0.1 convert_element_type.34
  8.5 1.5 pad_maximum_fusion
  10.0 0.0 all-gather.6.cloned.1.call-update
  10.0 0.0 all-gather.10.cloned.1.call-start
  10.1 1.1 copy.22
  11.2 0.2 copy.24
  11.4 49.9 %all-gather.8.cloned.1.call-done = bf16[4096,256]{1,0:T(8,128)(2,1)} async-done(((bf16[512,256]{1,0:T(8,128)(2,1)}), bf16[4096,256]{1,0:T(8,128)(2,1)}) %all-gather.8.cloned.1.call-update) | async-done | bytes 2097168 | tf_op jit(solution)/shard_map/all_gather | solution.py:27
  61.3 4.0 reshape.64
  65.3 71.2 %all-gather.6.cloned.1.call-done = f32[4096,258]{0,1:T(8,128)} async-done(((f32[512,258]{0,1:T(8,128)}), f32[4096,258]{0,1:T(8,128)}) %all-gather.6.cloned.1.call-update) | async-done | bytes 4227088 | tf_op jit(solution)/shard_map/all_gather | solution.py:23
  136.5 0.0 slice-start
  136.5 2.7 split.8
  139.2 2.8 reshape.65
  142.0 0.0 copy-done
  142.0 0.0 slice-done
  142.0 63.3 %while.15 = (s32[]{:T(128)}, f32[512,2]{0,1:T(2,128)S(1)}, f32[512,2]{0,1:T(2,128)S(1)}, f32[512,2,128]{0,2,1:T(8,128)}, s32[2]{0:T(128)S(1)}, /*index=5*/bf16[2...) while((s32[]{:T(128)}, f32[512,2]{0,1:T(2,128)S(1)}, ...), condition=%wide.region_3.4_spmd.clone, body=%wide.region_0.3_spmd.clone.sunk | while | flops 1110842880 | bytes 41337040 | solution.py:58
  142.0 0.6 dynamic_slice.29
  144.4 0.1 dynamic-slice_bitcast_fusion.2
  144.5 0.6 iota_add_fusion.5
  145.1 0.8 broadcast_compare_fusion.2
  145.9 3.8 constant_dynamic-slice_fusion.4
  149.7 3.6 copy.36
  153.2 6.6 %fusion.41 = (f32[512,2]{0,1:T(2,128)S(1)}, f32[2,2048,512]{2,1,0:T(8,128)}) fusion(f32[2,2048]{1,0:T(2,128)S(1)} %dynamic-slice_bitcast_fusion.2, f32[512,2]{0,1:T(2,128)S(1)} %get-tuple-element.264, pred[512,2048]{0,1:T(8,128)(4,1)S(1)} %broadcast_compare_fusion.2, bf16[512,2,128]{2,0,1:T(8,128)(2,1)S(1)} %get-tuple-element.263, ...), kind=kOutput, calls=%fused_computation.7.clone.1 | convolution fusion | flops 547355648 | bytes 10772480 | tf_op jit(solution)/shard_map/while/body/eval_jaxpr/qhd,khd->qhk/dot_general | solution.py:39
  159.9 4.8 fusion.43
  164.7 1.8 constant_dynamic-slice_fusion.5
  166.5 0.8 copy.37
  167.3 6.2 %fusion.45 = f32[512,2,128]{0,2,1:T(8,128)} fusion(f32[2,2048,512]{2,1,0:T(8,128)} %get-tuple-element.226, f32[512,2]{0,1:T(2,128)S(1)} %fusion.42, f32[2,2048]{1,0:T(2,128)S(1)} %dynamic-slice_bitcast_fusion.2, f32[512,2]{0,1:T(2,128)S(1)} %get-tuple-element.264, pred[512,2048]{0,1:T(8,128)(4,1)S(1)} %broadcast_compare_fusion.2, ...), kind=kOutput, calls=%fused_computation.14.clone.1 | convolution fusion | flops 549847040 | bytes 11563009 | tf_op jit(solution)/shard_map/while/body/eval_jaxpr/qhk,khd->qhd/dot_general | solution.py:49
  173.6 0.6 dynamic_slice.29
  176.0 0.1 dynamic-slice_bitcast_fusion.2
  176.1 0.6 iota_add_fusion.5
  176.7 0.8 broadcast_compare_fusion.2
  177.5 3.8 constant_dynamic-slice_fusion.4
  181.2 3.6 copy.36
  184.8 6.6 %fusion.41 = (f32[512,2]{0,1:T(2,128)S(1)}, f32[2,2048,512]{2,1,0:T(8,128)}) fusion(f32[2,2048]{1,0:T(2,128)S(1)} %dynamic-slice_bitcast_fusion.2, f32[512,2]{0,1:T(2,128)S(1)} %get-tuple-element.264, pred[512,2048]{0,1:T(8,128)(4,1)S(1)} %broadcast_compare_fusion.2, bf16[512,2,128]{2,0,1:T(8,128)(2,1)S(1)} %get-tuple-element.263, ...), kind=kOutput, calls=%fused_computation.7.clone.1 | convolution fusion | flops 547355648 | bytes 10772480 | tf_op jit(solution)/shard_map/while/body/eval_jaxpr/qhd,khd->qhk/dot_general | solution.py:39
  191.5 4.8 fusion.43
  196.3 1.8 constant_dynamic-slice_fusion.5
  198.1 0.8 copy.37
  198.9 6.4 %fusion.45 = f32[512,2,128]{0,2,1:T(8,128)} fusion(f32[2,2048,512]{2,1,0:T(8,128)} %get-tuple-element.226, f32[512,2]{0,1:T(2,128)S(1)} %fusion.42, f32[2,2048]{1,0:T(2,128)S(1)} %dynamic-slice_bitcast_fusion.2, f32[512,2]{0,1:T(2,128)S(1)} %get-tuple-element.264, pred[512,2048]{0,1:T(8,128)(4,1)S(1)} %broadcast_compare_fusion.2, ...), kind=kOutput, calls=%fused_computation.14.clone.1 | convolution fusion | flops 549847040 | bytes 11563009 | tf_op jit(solution)/shard_map/while/body/eval_jaxpr/qhk,khd->qhd/dot_general | solution.py:49
  205.3 0.0 copy-start.1
  205.3 1.1 divide_convert_fusion
  206.4 0.1 reshape.66
  206.4 0.2 copy.31
  206.6 8.5 %all_to_all.16 = bf16[4,128,256]{2,1,0:T(8,128)(2,1)S(1)} all-to-all(bf16[4,128,256]{2,1,0:T(8,128)(2,1)S(1)} %copy.31), channel_id=1, replica_groups=mesh['sp'=8,'tp'=4] {'tp'}, dimensions={0} | all-to-all | bytes 524288 | tf_op jit(solution)/shard_map/all_to_all | solution.py:61
  215.2 0.2 copy.27
  215.3 3.1 multiply_reduce_fusion
  218.5 0.0 copy-done.1
  218.5 0.9 multiply_convert_fusion.1
  219.4 0.0 all-gather.10.cloned.1.call-update
  219.5 0.0 all-gather.12.cloned.1.call-start
  219.5 0.5 all-gather.12.cloned.1.call-update
  220.0 0.0 all-gather.14.cloned.1.call-start
  220.1 0.5 all-gather.14.cloned.1.call-update
  220.6 0.0 reduce-scatter.2.cloned.1.call-start
  220.7 19.1 %all-gather.10.cloned.1.call-done = bf16[512,2048]{1,0:T(8,128)(2,1)} async-done(((bf16[128,2048]{1,0:T(8,128)(2,1)}), bf16[512,2048]{1,0:T(8,128)(2,1)}) %all-gather.10.cloned.1.call-update) | async-done | bytes 2097168 | tf_op jit(solution)/shard_map/all_gather | solution.py:66
  239.8 126.5 %all-gather.12.cloned.1.call-done = bf16[2048,2048]{1,0:T(8,128)(2,1)} async-done(((bf16[256,2048]{1,0:T(8,128)(2,1)}), bf16[2048,2048]{1,0:T(8,128)(2,1)}) %all-gather.12.cloned.1.call-update) | async-done | bytes 8388624 | tf_op jit(solution)/shard_map/all_gather | solution.py:69
  366.3 125.0 %all-gather.14.cloned.1.call-done = bf16[2048,2048]{1,0:T(8,128)(2,1)} async-done(((bf16[2048,256]{1,0:T(8,128)(2,1)}), bf16[2048,2048]{1,0:T(8,128)(2,1)}) %all-gather.14.cloned.1.call-update) | async-done | bytes 8388624 | tf_op jit(solution)/shard_map/all_gather | solution.py:73
  491.3 16.5 %convolution_convert_fusion = bf16[512,2048]{1,0:T(8,128)(2,1)} fusion(bf16[2048,2048]{1,0:T(8,128)(2,1)} %all-gather.14.cloned.1.call-done, bf16[512,2048]{1,0:T(8,128)(2,1)} %all-gather.10.cloned.1.call-done, bf16[2048,2048]{1,0:T(8,128)(2,1)} %all-gather.12.cloned.1.call-done), kind=kOutput, calls=%fused_computation.30 | convolution fusion | flops 8594128896 | bytes 20971520 | tf_op jit(solution)/shard_map/dot_general | solution.py:74
  507.8 0.0 reduce-scatter.2.cloned.1.call-update
  507.9 29.5 %reduce-scatter.2.cloned.1.call-done = bf16[128,2048]{1,0:T(8,128)(2,1)} async-done(((bf16[512,2048]{1,0:T(8,128)(2,1)}), bf16[128,2048]{1,0:T(8,128)(2,1)}) %reduce-scatter.2.cloned.1.call-update) | async-done | bytes 524304 | tf_op jit(solution)/shard_map/reduce_scatter | solution.py:75
  537.3 1.9 add_convert_fusion
  (13 shorter events, 0.1 us)
Async XLA Ops:
  6.5 54.8 %all-gather.8.cloned.1.call-start = ((), (), s32[]{:S(2)}) async-start(), calls=%async_computation.3 | async-start | bytes 2359296 | tf_op jit(solution)/shard_map/all_gather | solution.py:27
  6.5 135.4 %copy-start = (f32[512,2]{0,1:T(2,128)S(1)}, f32[512,2]{0,1:T(2,128)}, u32[]{:S(2)}) copy-start(f32[512,2]{0,1:T(2,128)} %param.14) | copy-start | bytes 12292
  7.3 129.2 %all-gather.6.cloned.1.call-start = ((), (), s32[]{:S(2)}) async-start(), calls=%async_computation.2 | async-start | bytes 4866048 | tf_op jit(solution)/shard_map/all_gather | solution.py:23
  10.0 229.7 %all-gather.10.cloned.1.call-start = ((), (), s32[]{:S(2)}) async-start(), calls=%async_computation.4 | async-start | bytes 2621440 | tf_op jit(solution)/shard_map/all_gather | solution.py:66
  136.5 5.5 %slice-start = ((f32[4096,258]{0,1:T(8,128)}), f32[4096,2]{0,1:T(2,128)S(1)}, s32[]{:S(2)}) async-start(f32[4096,258]{0,1:T(8,128)} %all-gather.6.cloned.1.call-done), calls=%async_computation.8 | async-start | bytes 65536 | tf_op jit(solution)/shard_map/split | solution.py:22
  205.3 13.2 %copy-start.1 = (f32[2048]{0:T(1024)S(1)}, f32[2048]{0:T(1024)}, u32[]{:S(2)}) copy-start(f32[2048]{0:T(1024)} %param.17) | copy-start | bytes 24580
  219.5 146.8 %all-gather.12.cloned.1.call-start = ((), (), s32[]{:S(2)}) async-start(), calls=%async_computation.5 | async-start | bytes 9437184 | tf_op jit(solution)/shard_map/all_gather | solution.py:69
  220.0 271.3 %all-gather.14.cloned.1.call-start = ((), (), s32[]{:S(2)}) async-start(), calls=%async_computation.6 | async-start | bytes 9437184 | tf_op jit(solution)/shard_map/all_gather | solution.py:73
  220.6 316.7 %reduce-scatter.2.cloned.1.call-start = ((), (), s32[]{:S(2)}) async-start(), calls=%async_computation.7 | async-start | bytes 2621440 | tf_op jit(solution)/shard_map/reduce_scatter | solution.py:75
Sparse Core Ops, SparseCore 0:
  9.5 51.7 all-gather.7
  63.5 72.9 all-gather.5
  219.6 20.1 all-gather.9
  241.8 124.4 all-gather.11
  368.2 123.1 all-gather.13
  508.0 29.3 reduce-scatter.1
